TPU v7x, 32 devices: a whole 2x2x4 slice. The times are simulated.
32 devices in a mesh: grp: 2 (over y), fs: 4 (over z), tp: 4 (over x, core).
Axes of the slice: x: 2, y: 2, z: 4, core: 2. Of those that a mesh axis runs over, the one named last changes fastest.
Arguments:
- prompt: bfloat16 [8, 1024, 2048], P(('grp', 'tp')), parts along dimension 0, may hold values from -6 to 6
- gate_first: float32 [2048, 5632], P('fs', 'tp'), may hold values from -0.125 to 0.125
- up_first: float32 [2048, 5632], P('fs', 'tp'), may hold values from -0.125 to 0.125
- down_first: float32 [5632, 2048], P('fs', 'tp'), may hold values from -0.3125 to 0.3125
- norm_gain: float32 [2048], replicated, may hold values from 0.1 to 1.9
- gate_second: float32 [2048, 5632], P('fs', 'tp'), may hold values from -0.125 to 0.125
- up_second: float32 [2048, 5632], P('fs', 'tp'), may hold values from -0.125 to 0.125
- down_second: float32 [5632, 2048], P('fs', 'tp'), may hold values from -0.3125 to 0.3125
Outputs:
- result: bfloat16 [8, 1024, 2048], P(('grp', 'tp'), 'fs'), parts along dimension 0
- gate_one: bfloat16 [4096, 5632], P('grp', 'fs'), parts along dimension 0
- up_one: bfloat16 [4096, 5632], P('grp', 'fs'), parts along dimension 0
- down_one: bfloat16 [5632, 4096], P('fs', 'grp'), parts along dimension 1
- gate_two: bfloat16 [4096, 5632], P('grp', 'fs'), parts along dimension 0
- up_two: bfloat16 [4096, 5632], P('grp', 'fs'), parts along dimension 0
- down_two: bfloat16 [5632, 4096], P('fs', 'grp'), parts along dimension 1
There are 2 independent parts, one for each index of `grp`. A program takes and returns all parts, laid end to end along the dimension named above; an argument that names none is the same for every part. Nothing has to cross between parts.
All inputs are finite; a program needn't handle non-finite values.
Results may differ from a plain program's by a relative error of at most 0.029.
Values may be sent and summed in bfloat16 or wider, within the bound.
A program may use at most 192 MiB of HBM per device.

v0:
```python
import jax
import jax.numpy as jnp
from jax import lax
from jax.sharding import PartitionSpec as P

norm_eps = 1e-05
deep_alpha = 2.0**0.25
half_step = 0.5


def plain_norm(values):
    row_mean = jnp.mean(values, axis=-1, keepdims=True)
    centred = values - row_mean
    variance = jnp.mean(centred * centred, axis=-1, keepdims=True)
    return centred * lax.rsqrt(variance + norm_eps)


def gated_hidden(inputs, gate_proj, up_proj):
    gate_act = jnp.dot(inputs, gate_proj, preferred_element_type=jnp.float32)
    up_act = jnp.dot(inputs, up_proj, preferred_element_type=jnp.float32)
    return (jax.nn.silu(gate_act) * up_act).astype(jnp.bfloat16)


def relay_weights(gate_proj, up_proj, down_proj):
    gate_rows, up_rows, down_mine = (
        lax.all_gather(gate_proj, "tp", axis=1, tiled=True),
        lax.all_gather(up_proj, "tp", axis=1, tiled=True),
        lax.all_gather(down_proj, "tp", axis=1, tiled=True),
    )
    gate_mine, up_mine = (
        lax.all_to_all(gate_rows, "fs", split_axis=1, concat_axis=0, tiled=True),
        lax.all_to_all(up_rows, "fs", split_axis=1, concat_axis=0, tiled=True),
    )
    return (gate_mine, up_mine, down_mine)


def row_terms(hidden, down_proj):
    return jnp.dot(hidden, down_proj, preferred_element_type=jnp.float32)


def body(prompt, gate_first, up_first, down_first, norm_gain, gate_second, up_second, down_second):
    fs_index = lax.axis_index("fs")
    row_block = gate_first.shape[0]
    gain_rows = lax.dynamic_slice_in_dim(norm_gain, fs_index * row_block, row_block, 0)
    gate_one, up_one, down_one = relay_weights(
        gate_first.astype(jnp.bfloat16),
        up_first.astype(jnp.bfloat16),
        down_first.astype(jnp.bfloat16),
    )
    gate_two, up_two, down_two = relay_weights(
        (gain_rows[:, None] * gate_second).astype(jnp.bfloat16),
        (gain_rows[:, None] * up_second).astype(jnp.bfloat16),
        down_second.astype(jnp.bfloat16),
    )
    tokens = prompt.reshape(-1, prompt.shape[-1])
    own_count = tokens.shape[0] // lax.axis_size("fs")
    own_first = fs_index * own_count
    hidden_one = gated_hidden(tokens, gate_one, up_one)
    own_tokens = lax.dynamic_slice_in_dim(tokens, own_first, own_count, 0)
    ffn_one = lax.psum_scatter(
        row_terms(hidden_one, down_one).astype(jnp.bfloat16), "fs", scatter_dimension=0, tiled=True
    ).astype(jnp.float32)
    normed_own = plain_norm(
        deep_alpha * own_tokens.astype(jnp.float32) + half_step * ffn_one
    ).astype(jnp.bfloat16)
    hidden_two = gated_hidden(
        lax.all_gather(normed_own, "fs", axis=0, tiled=True), gate_two, up_two
    )
    ffn_two = lax.psum_scatter(
        row_terms(hidden_two, down_two).astype(jnp.bfloat16), "fs", scatter_dimension=0, tiled=True
    ).astype(jnp.float32)
    residual_two = deep_alpha * norm_gain * normed_own.astype(jnp.float32)
    result = plain_norm(residual_two + half_step * ffn_two).astype(jnp.bfloat16)
    return (
        result.reshape(1, result.shape[0], result.shape[-1]),
        gate_one,
        up_one,
        down_one,
        gate_two,
        up_two,
        down_two,
    )


def solution(mesh):
    placed = (
        P(("grp", "tp"), None, None),
        P("fs", "tp"),
        P("fs", "tp"),
        P("fs", "tp"),
        P(),
        P("fs", "tp"),
        P("fs", "tp"),
        P("fs", "tp"),
    )
    return jax.shard_map(
        body,
        mesh=mesh,
        in_specs=placed,
        out_specs=(
            P(("grp", "tp"), "fs", None),
            P("grp", "fs"),
            P("grp", "fs"),
            P("fs", "grp"),
            P("grp", "fs"),
            P("grp", "fs"),
            P("fs", "grp"),
        ),
        check_vma=False,
    )
```

profile of v0, /device:TPU:0, one launch (start us, length us, event | category | flops | bytes accessed | tf_op | source)
XLA Modules:
  0.0 934.5 jit_solution(12915030123418314235)
XLA Ops:
  11.8 44.9 %all-gather.8.cloned.1.call-done = bf16[512,5632]{1,0:T(8,128)(2,1)} async-done(((bf16[512,1408]{1,0:T(8,128)(2,1)}), bf16[512,5632]{1,0:T(8,128)(2,1)}) %all-gather.8.cloned.1.call-update) | async-done | bytes 5767184 | tf_op jit(solution)/shard_map/all_gather | solution.py:26
  56.7 5.6 copy.30
  62.3 5.5 all-to-all-start
  69.2 33.0 %all-gather.10.cloned.1.call-done = bf16[512,5632]{1,0:T(8,128)(2,1)} async-done(((bf16[512,1408]{1,0:T(8,128)(2,1)}), bf16[512,5632]{1,0:T(8,128)(2,1)}) %all-gather.10.cloned.1.call-update) | async-done | bytes 5767184 | tf_op jit(solution)/shard_map/all_gather | solution.py:27
  102.2 5.6 copy.29
  107.8 87.6 %all-to-all-done = bf16[512,4,1408]{2,0,1:T(8,128)(2,1)} async-done(((bf16[512,4,1408]{2,0,1:T(8,128)(2,1)}), bf16[512,4,1408]{2,0,1:T(8,128)(2,1)}, u32[]{:S(2)}, u32[]{:S(2)}) %all-to-all-start) | async-done | bytes 5767200 | tf_op jit(solution)/shard_map/all_to_all | solution.py:31
  195.4 5.5 all-to-all-start.1
  205.1 11.7 %fusion.1 = f32[1024,1408]{1,0:T(8,128)} fusion(bf16[2048,1408]{1,0:T(8,128)(2,1)} %bitcast.3, bf16[1,1024,2048]{2,1,0:T(8,128)(2,1)} %param.8), kind=kOutput, calls=%fused_computation.7 | convolution fusion | flops 5905580032 | bytes 15728640 | tf_op jit(solution)/shard_map/dot_general | solution.py:19
  216.8 110.9 %all-to-all-done.1 = bf16[512,4,1408]{2,0,1:T(8,128)(2,1)} async-done(((bf16[512,4,1408]{2,0,1:T(8,128)(2,1)}), bf16[512,4,1408]{2,0,1:T(8,128)(2,1)}, u32[]{:S(2)}, u32[]{:S(2)}) %all-to-all-start.1) | async-done | bytes 5767200 | tf_op jit(solution)/shard_map/all_to_all | solution.py:32
  327.7 20.6 %convolution_convert_fusion.1 = bf16[1024,2048]{1,0:T(8,128)(2,1)} fusion(bf16[1408,2048]{1,0:T(8,128)(2,1)} %all-gather.12.cloned.1.call-done, f32[1024,1408]{1,0:T(8,128)} %fusion.1, bf16[2048,1408]{1,0:T(8,128)(2,1)} %bitcast.5, bf16[1,1024,2048]{2,1,0:T(8,128)(2,1)} %param.8), kind=kOutput, calls=%fused_computation.10 | convolution fusion | flops 11821907968 | bytes 25690112 | tf_op jit(solution)/shard_map/dot_general | solution.py:38
  348.9 5.6 copy.28
  359.7 124.0 %reduce-scatter.3.cloned.1.call-done = bf16[256,2048]{1,0:T(8,128)(2,1)} async-done(((bf16[1024,2048]{1,0:T(8,128)(2,1)}), bf16[256,2048]{1,0:T(8,128)(2,1)}) %reduce-scatter.3.cloned.1.call-update) | async-done | bytes 1048592 | tf_op jit(solution)/shard_map/reduce_scatter | solution.py:60
  492.3 82.7 %all-gather.18.cloned.1.call-done = bf16[512,5632]{1,0:T(8,128)(2,1)} async-done(((bf16[512,1408]{1,0:T(8,128)(2,1)}), bf16[512,5632]{1,0:T(8,128)(2,1)}) %all-gather.18.cloned.1.call-update) | async-done | bytes 5767184 | tf_op jit(solution)/shard_map/all_gather | solution.py:27
  575.0 5.6 copy.27
  580.6 5.3 all-to-all-start.3
  585.9 167.0 %all-gather.14.cloned.1.call-done = bf16[1024,2048]{1,0:T(8,128)(2,1)} async-done(((bf16[256,2048]{1,0:T(8,128)(2,1)}), bf16[1024,2048]{1,0:T(8,128)(2,1)}) %all-gather.14.cloned.1.call-update) | async-done | bytes 4194320 | tf_op jit(solution)/shard_map/all_gather | solution.py:67
  753.0 11.7 %fusion.6 = f32[1024,1408]{1,0:T(8,128)} fusion(bf16[1024,2048]{1,0:T(8,128)(2,1)} %all-gather.14.cloned.1.call-done, bf16[2048,1408]{1,0:T(8,128)(2,1)} %bitcast.7), kind=kOutput, calls=%fused_computation.27 | convolution fusion | flops 5905580032 | bytes 15728640 | tf_op jit(solution)/shard_map/dot_general | solution.py:19
  764.7 32.5 %all-gather.20.cloned.1.call-done = bf16[1408,2048]{1,0:T(8,128)(2,1)} async-done(((bf16[1408,512]{1,0:T(8,128)(2,1)}), bf16[1408,2048]{1,0:T(8,128)(2,1)}) %all-gather.20.cloned.1.call-update) | async-done | bytes 5767184 | tf_op jit(solution)/shard_map/all_gather | solution.py:28
  797.2 20.6 %convolution_convert_fusion = bf16[1024,2048]{1,0:T(8,128)(2,1)} fusion(bf16[1408,2048]{1,0:T(8,128)(2,1)} %all-gather.20.cloned.1.call-done, f32[1024,1408]{1,0:T(8,128)} %fusion.6, bf16[1024,2048]{1,0:T(8,128)(2,1)} %all-gather.14.cloned.1.call-done, bf16[2048,1408]{1,0:T(8,128)(2,1)} %bitcast.9), kind=kOutput, calls=%fused_computation.9 | convolution fusion | flops 11821907968 | bytes 25690112 | tf_op jit(solution)/shard_map/dot_general | solution.py:38
  817.8 76.9 %reduce-scatter.5.cloned.1.call-done = bf16[256,2048]{1,0:T(8,128)(2,1)} async-done(((bf16[1024,2048]{1,0:T(8,128)(2,1)}), bf16[256,2048]{1,0:T(8,128)(2,1)}) %reduce-scatter.5.cloned.1.call-update) | async-done | bytes 1048592 | tf_op jit(solution)/shard_map/reduce_scatter | solution.py:69
  900.1 5.7 copy.37
  905.8 5.6 copy.38
  914.0 5.7 copy.40
  919.7 5.7 copy.41
  (68 shorter events, 34.9 us)
Async XLA Ops:
  7.2 49.5 %all-gather.8.cloned.1.call-start = ((), (), s32[]{:S(2)}) async-start(), calls=%async_computation.6 | async-start | bytes 7208960 | tf_op jit(solution)/shard_map/all_gather | solution.py:26
  10.5 91.8 %all-gather.10.cloned.1.call-start = ((), (), s32[]{:S(2)}) async-start(), calls=%async_computation.7 | async-start | bytes 7208960 | tf_op jit(solution)/shard_map/all_gather | solution.py:27
  62.3 5.6 copy-start.5
  62.3 133.1 %all-to-all-start = ((bf16[512,4,1408]{2,0,1:T(8,128)(2,1)}), bf16[512,4,1408]{2,0,1:T(8,128)(2,1)}, u32[]{:S(2)}, u32[]{:S(2)}) async-start(bf16[512,4,1408]{2,0,1:T(8,128)(2,1)} %bitcast.71), calls=%async_computation | async-start | bytes 11534336 | tf_op jit(solution)/shard_map/all_to_all | solution.py:31
  67.8 148.9 %all-gather.12.cloned.1.call-start = ((), (), s32[]{:S(2)}) async-start(), calls=%async_computation.8 | async-start | bytes 7208960 | tf_op jit(solution)/shard_map/all_gather | solution.py:28
  195.4 5.5 copy-start.7
  195.4 5.6 copy-start.3
  195.4 132.2 %all-to-all-start.1 = ((bf16[512,4,1408]{2,0,1:T(8,128)(2,1)}), bf16[512,4,1408]{2,0,1:T(8,128)(2,1)}, u32[]{:S(2)}, u32[]{:S(2)}) async-start(bf16[512,4,1408]{2,0,1:T(8,128)(2,1)} %bitcast.70), calls=%async_computation.1 | async-start | bytes 11534336 | tf_op jit(solution)/shard_map/all_to_all | solution.py:32
  200.9 147.9 %all-gather.16.cloned.1.call-start = ((), (), s32[]{:S(2)}) async-start(), calls=%async_computation.11 | async-start | bytes 7208960 | tf_op jit(solution)/shard_map/all_gather | solution.py:26
  205.0 278.6 %reduce-scatter.3.cloned.1.call-start = ((), (), s32[]{:S(2)}) async-start(), calls=%async_computation.9 | async-start | bytes 5242880 | tf_op jit(solution)/shard_map/reduce_scatter | solution.py:60
  348.2 226.7 %all-gather.18.cloned.1.call-start = ((), (), s32[]{:S(2)}) async-start(), calls=%async_computation.12 | async-start | bytes 7208960 | tf_op jit(solution)/shard_map/all_gather | solution.py:27
  354.5 226.1 %all-to-all-start.2 = ((bf16[512,4,1408]{2,0,1:T(8,128)(2,1)}), bf16[512,4,1408]{2,0,1:T(8,128)(2,1)}, u32[]{:S(2)}, u32[]{:S(2)}) async-start(bf16[512,4,1408]{2,0,1:T(8,128)(2,1)} %bitcast.69), calls=%async_computation.3 | async-start | bytes 11534336 | tf_op jit(solution)/shard_map/all_to_all | solution.py:31
  359.6 393.4 %all-gather.14.cloned.1.call-start = ((), (), s32[]{:S(2)}) async-start(), calls=%async_computation.10 | async-start | bytes 5242880 | tf_op jit(solution)/shard_map/all_gather | solution.py:67
  359.7 131.3 %copy-start.6 = (f32[1408,512]{1,0:T(8,128)S(1)}, f32[1408,512]{1,0:T(8,128)}, u32[]{:S(2)}) copy-start(f32[1408,512]{1,0:T(8,128)} %param.15) | copy-start | bytes 8650756
  483.7 4.3 copy-start.1
  490.8 306.4 %all-gather.20.cloned.1.call-start = ((), (), s32[]{:S(2)}) async-start(), calls=%async_computation.13 | async-start | bytes 7208960 | tf_op jit(solution)/shard_map/all_gather | solution.py:28
  580.6 216.6 %all-to-all-start.3 = ((bf16[512,4,1408]{2,0,1:T(8,128)(2,1)}), bf16[512,4,1408]{2,0,1:T(8,128)(2,1)}, u32[]{:S(2)}, u32[]{:S(2)}) async-start(bf16[512,4,1408]{2,0,1:T(8,128)(2,1)} %bitcast.72), calls=%async_computation.4 | async-start | bytes 11534336 | tf_op jit(solution)/shard_map/all_to_all | solution.py:32
  585.9 308.8 %reduce-scatter.5.cloned.1.call-start = ((), (), s32[]{:S(2)}) async-start(), calls=%async_computation.14 | async-start | bytes 5242880 | tf_op jit(solution)/shard_map/reduce_scatter | solution.py:69
  817.8 77.0 %copy-start = (bf16[256,2048]{1,0:T(8,128)(2,1)S(1)}, bf16[256,2048]{1,0:T(8,128)(2,1)}, u32[]{:S(2)}) copy-start(bf16[256,2048]{1,0:T(8,128)(2,1)} %multiply_convert_fusion.5) | copy-start | bytes 3145732
  894.7 3.8 copy-start.2
  896.6 14.9 %slice-start = ((s8[5767168]{0:T(1024)(128)(4,1)}), s8[4194304]{0:T(1024)(128)(4,1)S(1)}, s32[]{:S(2)}) async-start(s8[5767168]{0:T(1024)(128)(4,1)} %bitcast.73), calls=%async_computation.15 | async-start | bytes 8388608
  900.1 11.3 %slice-start.1 = ((s8[5767168]{0:T(1024)(128)(4,1)}), s8[1572864]{0:T(1024)(128)(4,1)S(1)}, s32[]{:S(2)}) async-start(s8[5767168]{0:T(1024)(128)(4,1)} %bitcast.73), calls=%async_computation.16 | async-start | bytes 3145728
  913.9 11.5 %slice-start.2 = ((s8[5767168]{0:T(1024)(128)(4,1)}), s8[4194304]{0:T(1024)(128)(4,1)S(1)}, s32[]{:S(2)}) async-start(s8[5767168]{0:T(1024)(128)(4,1)} %bitcast.75), calls=%async_computation.17 | async-start | bytes 8388608
  919.7 5.7 slice-start.3
  (1 other events, 3.3 us)
Sparse Core Ops, SparseCore 0:
  10.6 46.0 all-gather.7
  58.8 43.3 all-gather.9
  104.4 43.3 all-gather.11
  205.2 43.7 all-gather.15
  348.4 135.2 reduce-scatter.2
  485.7 89.2 all-gather.17
  577.1 175.8 all-gather.13
  755.1 42.0 all-gather.19
  817.9 76.7 reduce-scatter.4
where the time goes:
time: 935 us; the launch traced here: 934 us
  waiting for transfers between devices  760 us (81%)
  matrix products  64.5 us (7%)
  local copies, waits for them, and re-layouts  50.3 us (5%)
  other arithmetic  23.4 us (3%)
  starting transfers between devices  22.1 us (2%)
  between operations  14 us (1%)
    all_gather x1, waiting for transfers between devices, body(): lax.all_gather(normed_own, 'fs', axis=0, tiled=True)  167 us
    reduce_scatter x1, waiting for transfers between devices, body(): lax.psum_scatter(row_terms(hidden_one, down_one).astype(jnp.bfloat16), 'f...  124 us
    all_gather x2, waiting for transfers between devices, relay_weights(): lax.all_gather(up_proj, 'tp', axis=1, tiled=True)  116 us
    all_to_all x2, waiting for transfers between devices, relay_weights(): lax.all_to_all(up_rows, 'fs', split_axis=1, concat_axis=0, tiled=True)  111 us
    all_to_all x2, waiting for transfers between devices, relay_weights(): lax.all_to_all(gate_rows, 'fs', split_axis=1, concat_axis=0, tiled=True)  87.6 us
    reduce_scatter x1, waiting for transfers between devices, body(): lax.psum_scatter(row_terms(hidden_two, down_two).astype(jnp.bfloat16), 'f...  76.9 us
    all_gather x2, waiting for transfers between devices, relay_weights(): lax.all_gather(gate_proj, 'tp', axis=1, tiled=True)  44.9 us
    dot_general x2, matrix products, row_terms(): return jnp.dot(hidden, down_proj, preferred_element_type=jnp.float32)  41.1 us
  transfers between devices with their start and end apart: 13, of which 9 were waited for; matrix products, arithmetic and copies ran while one was open for 9% of the time, Pallas kernels for 0%

commit v1 on v0

--- a/solution.py
+++ b/solution.py
@@ -2,10 +2,17 @@
 import jax.numpy as jnp
 from jax import lax
 from jax.sharding import PartitionSpec as P
+from jax.lax import all_gather
 
 norm_eps = 1e-05
 deep_alpha = 2.0**0.25
 half_step = 0.5
+
+
+def measure_zones(m):
+    taken_in = all_gather(m, "tp")
+    prior = jnp.concatenate(taken_in, 1)
+    return prior
 
 
 def plain_norm(values):
@@ -24,7 +31,7 @@
 def relay_weights(gate_proj, up_proj, down_proj):
     gate_rows, up_rows, down_mine = (
         lax.all_gather(gate_proj, "tp", axis=1, tiled=True),
-        lax.all_gather(up_proj, "tp", axis=1, tiled=True),
+        measure_zones(up_proj),
         lax.all_gather(down_proj, "tp", axis=1, tiled=True),
     )
     gate_mine, up_mine = (

time: 935 us -> 935 us (level)
  waiting for transfers between devices: 760 us -> 772 us
  local copies, waits for them, and re-layouts: 50.3 us -> 39.3 us
    all_to_all x2 -> x0, local copies, waits for them, and re-layouts: 11.2 us -> none  [relay_weights(): lax.all_to_all(up_rows, 'fs', split_axis=1, concat_axis=0, tiled=True)]
  transfers between devices with their start and end apart: 13 -> 13, of which waited for: 9 -> 9; matrix products, arithmetic and copies ran while one was open for 9% -> 7% of each run, Pallas kernels for 0% -> 0%
where the time goes in v1:
time: 935 us; the launch traced here: 934 us
  waiting for transfers between devices  772 us (83%)
  matrix products  64.5 us (7%)
  local copies, waits for them, and re-layouts  39.3 us (4%)
  other arithmetic  23.2 us (2%)
  starting transfers between devices  21.9 us (2%)
  between operations  14 us (1%)
    all_gather x1, waiting for transfers between devices, body(): lax.all_gather(normed_own, 'fs', axis=0, tiled=True)  168 us
    reduce_scatter x1, waiting for transfers between devices, body(): lax.psum_scatter(row_terms(hidden_one, down_one).astype(jnp.bfloat16), 'f...  124 us
    all_gather x2, waiting for transfers between devices, measure_zones(): taken_in = all_gather(m, 'tp')  116 us
    all_to_all x2, waiting for transfers between devices, relay_weights(): lax.all_to_all(up_rows, 'fs', split_axis=1, concat_axis=0, tiled=True)  111 us
    all_to_all x2, waiting for transfers between devices, relay_weights(): lax.all_to_all(gate_rows, 'fs', split_axis=1, concat_axis=0, tiled=True)  93.2 us
    reduce_scatter x1, waiting for transfers between devices, body(): lax.psum_scatter(row_terms(hidden_two, down_two).astype(jnp.bfloat16), 'f...  76.9 us
    all_gather x2, waiting for transfers between devices, relay_weights(): lax.all_gather(gate_proj, 'tp', axis=1, tiled=True)  44.9 us
    dot_general x2, matrix products, row_terms(): return jnp.dot(hidden, down_proj, preferred_element_type=jnp.float32)  41.1 us
  transfers between devices with their start and end apart: 13, of which 9 were waited for; matrix products, arithmetic and copies ran while one was open for 7% of the time, Pallas kernels for 0%

profile of v1, /device:TPU:0, one launch (start us, length us, event | category | flops | bytes accessed | tf_op | source)
XLA Modules:
  0.0 934.5 jit_solution(7914213906517003144)
XLA Ops:
  11.8 44.9 %all-gather.10.cloned.1.call-done = bf16[512,5632]{1,0:T(8,128)(2,1)} async-done(((bf16[512,1408]{1,0:T(8,128)(2,1)}), bf16[512,5632]{1,0:T(8,128)(2,1)}) %all-gather.10.cloned.1.call-update) | async-done | bytes 5767184 | tf_op jit(solution)/shard_map/all_gather | solution.py:33
  56.7 5.6 copy.22
  62.3 5.5 all-to-all-start
  69.2 33.0 %all-gather.20.cloned.1.call-done = bf16[2048,1408]{1,0:T(8,128)(2,1)} async-done(((bf16[512,1408]{1,0:T(8,128)(2,1)}), bf16[2048,1408]{1,0:T(8,128)(2,1)}) %all-gather.20.cloned.1.call-update) | async-done | bytes 5767184 | tf_op jit(solution)/shard_map/all_gather | solution.py:13
  102.2 93.2 %all-to-all-done = bf16[512,4,1408]{2,0,1:T(8,128)(2,1)} async-done(((bf16[512,4,1408]{2,0,1:T(8,128)(2,1)}), bf16[512,4,1408]{2,0,1:T(8,128)(2,1)}, u32[]{:S(2)}, u32[]{:S(2)}) %all-to-all-start) | async-done | bytes 5767200 | tf_op jit(solution)/shard_map/all_to_all | solution.py:38
  195.4 5.5 all-to-all-start.1
  201.1 3.9 multiply_convert_fusion.2
  205.1 11.7 %fusion.1 = f32[1024,1408]{1,0:T(8,128)} fusion(bf16[2048,1408]{1,0:T(8,128)(2,1)} %bitcast.3, bf16[1,1024,2048]{2,1,0:T(8,128)(2,1)} %param.8), kind=kOutput, calls=%fused_computation.5 | convolution fusion | flops 5905580032 | bytes 15728640 | tf_op jit(solution)/shard_map/dot_general | solution.py:26
  216.8 110.9 %all-to-all-done.1 = bf16[512,4,1408]{2,0,1:T(8,128)(2,1)} async-done(((bf16[512,4,1408]{2,0,1:T(8,128)(2,1)}), bf16[512,4,1408]{2,0,1:T(8,128)(2,1)}, u32[]{:S(2)}, u32[]{:S(2)}) %all-to-all-start.1) | async-done | bytes 5767200 | tf_op jit(solution)/shard_map/all_to_all | solution.py:39
  327.7 20.6 %convolution_convert_fusion.1 = bf16[1024,2048]{1,0:T(8,128)(2,1)} fusion(bf16[1408,2048]{1,0:T(8,128)(2,1)} %all-gather.12.cloned.1.call-done, f32[1024,1408]{1,0:T(8,128)} %fusion.1, bf16[2048,1408]{1,0:T(8,128)(2,1)} %bitcast.7, bf16[1,1024,2048]{2,1,0:T(8,128)(2,1)} %param.8), kind=kOutput, calls=%fused_computation.8 | convolution fusion | flops 11821907968 | bytes 25690112 | tf_op jit(solution)/shard_map/dot_general | solution.py:45
  348.9 5.6 copy.21
  354.5 5.2 all-to-all-start.2
  359.7 124.0 %reduce-scatter.3.cloned.1.call-done = bf16[256,2048]{1,0:T(8,128)(2,1)} async-done(((bf16[1024,2048]{1,0:T(8,128)(2,1)}), bf16[256,2048]{1,0:T(8,128)(2,1)}) %reduce-scatter.3.cloned.1.call-update) | async-done | bytes 1048592 | tf_op jit(solution)/shard_map/reduce_scatter | solution.py:67
  492.1 82.8 %all-gather.22.cloned.1.call-done = bf16[2048,1408]{1,0:T(8,128)(2,1)} async-done(((bf16[512,1408]{1,0:T(8,128)(2,1)}), bf16[2048,1408]{1,0:T(8,128)(2,1)}) %all-gather.22.cloned.1.call-update) | async-done | bytes 5767184 | tf_op jit(solution)/shard_map/all_gather | solution.py:13
  575.0 5.2 all-to-all-start.3
  580.4 167.9 %all-gather.14.cloned.1.call-done = bf16[1024,2048]{1,0:T(8,128)(2,1)} async-done(((bf16[256,2048]{1,0:T(8,128)(2,1)}), bf16[1024,2048]{1,0:T(8,128)(2,1)}) %all-gather.14.cloned.1.call-update) | async-done | bytes 4194320 | tf_op jit(solution)/shard_map/all_gather | solution.py:74
  748.3 11.7 %fusion.6 = f32[1024,1408]{1,0:T(8,128)} fusion(bf16[1024,2048]{1,0:T(8,128)(2,1)} %all-gather.14.cloned.1.call-done, bf16[2048,1408]{1,0:T(8,128)(2,1)} %bitcast.9), kind=kOutput, calls=%fused_computation.25 | convolution fusion | flops 5905580032 | bytes 15728640 | tf_op jit(solution)/shard_map/dot_general | solution.py:26
  760.0 37.2 %all-gather.18.cloned.1.call-done = bf16[1408,2048]{1,0:T(8,128)(2,1)} async-done(((bf16[1408,512]{1,0:T(8,128)(2,1)}), bf16[1408,2048]{1,0:T(8,128)(2,1)}) %all-gather.18.cloned.1.call-update) | async-done | bytes 5767184 | tf_op jit(solution)/shard_map/all_gather | solution.py:35
  797.2 20.6 %convolution_convert_fusion = bf16[1024,2048]{1,0:T(8,128)(2,1)} fusion(bf16[1408,2048]{1,0:T(8,128)(2,1)} %all-gather.18.cloned.1.call-done, f32[1024,1408]{1,0:T(8,128)} %fusion.6, bf16[1024,2048]{1,0:T(8,128)(2,1)} %all-gather.14.cloned.1.call-done, bf16[2048,1408]{1,0:T(8,128)(2,1)} %bitcast.13), kind=kOutput, calls=%fused_computation.7 | convolution fusion | flops 11821907968 | bytes 25690112 | tf_op jit(solution)/shard_map/dot_general | solution.py:45
  817.8 76.9 %reduce-scatter.5.cloned.1.call-done = bf16[256,2048]{1,0:T(8,128)(2,1)} async-done(((bf16[1024,2048]{1,0:T(8,128)(2,1)}), bf16[256,2048]{1,0:T(8,128)(2,1)}) %reduce-scatter.5.cloned.1.call-update) | async-done | bytes 1048592 | tf_op jit(solution)/shard_map/reduce_scatter | solution.py:76
  899.9 5.7 copy.29
  905.7 5.7 copy.30
  913.9 5.7 copy.32
  919.7 5.7 copy.33
  (66 shorter events, 25.7 us)
Async XLA Ops:
  7.2 49.5 %all-gather.10.cloned.1.call-start = ((), (), s32[]{:S(2)}) async-start(), calls=%async_computation.6 | async-start | bytes 7208960 | tf_op jit(solution)/shard_map/all_gather | solution.py:33
  10.5 91.8 %all-gather.20.cloned.1.call-start = ((), (), s32[]{:S(2)}) async-start(), calls=%async_computation.13 | async-start | bytes 7208960 | tf_op jit(solution)/shard_map/all_gather | solution.py:13
  62.3 5.6 copy-start.5
  62.3 133.1 %all-to-all-start = ((bf16[512,4,1408]{2,0,1:T(8,128)(2,1)}), bf16[512,4,1408]{2,0,1:T(8,128)(2,1)}, u32[]{:S(2)}, u32[]{:S(2)}) async-start(bf16[512,4,1408]{2,0,1:T(8,128)(2,1)} %bitcast.68), calls=%async_computation | async-start | bytes 11534336 | tf_op jit(solution)/shard_map/all_to_all | solution.py:38
  67.9 148.9 %all-gather.12.cloned.1.call-start = ((), (), s32[]{:S(2)}) async-start(), calls=%async_computation.7 | async-start | bytes 7208960 | tf_op jit(solution)/shard_map/all_gather | solution.py:35
  195.4 5.5 copy-start.7
  195.4 5.6 copy-start.3
  195.4 132.2 %all-to-all-start.1 = ((bf16[512,4,1408]{2,0,1:T(8,128)(2,1)}), bf16[512,4,1408]{2,0,1:T(8,128)(2,1)}, u32[]{:S(2)}, u32[]{:S(2)}) async-start(bf16[512,4,1408]{2,0,1:T(8,128)(2,1)} %bitcast.72), calls=%async_computation.1 | async-start | bytes 11534336 | tf_op jit(solution)/shard_map/all_to_all | solution.py:39
  200.9 147.9 %all-gather.16.cloned.1.call-start = ((), (), s32[]{:S(2)}) async-start(), calls=%async_computation.10 | async-start | bytes 7208960 | tf_op jit(solution)/shard_map/all_gather | solution.py:33
  205.0 278.6 %reduce-scatter.3.cloned.1.call-start = ((), (), s32[]{:S(2)}) async-start(), calls=%async_computation.8 | async-start | bytes 5242880 | tf_op jit(solution)/shard_map/reduce_scatter | solution.py:67
  348.2 226.7 %all-gather.22.cloned.1.call-start = ((), (), s32[]{:S(2)}) async-start(), calls=%async_computation.14 | async-start | bytes 7208960 | tf_op jit(solution)/shard_map/all_gather | solution.py:13
  354.5 220.5 %all-to-all-start.2 = ((bf16[512,4,1408]{2,0,1:T(8,128)(2,1)}), bf16[512,4,1408]{2,0,1:T(8,128)(2,1)}, u32[]{:S(2)}, u32[]{:S(2)}) async-start(bf16[512,4,1408]{2,0,1:T(8,128)(2,1)} %bitcast.67), calls=%async_computation.3 | async-start | bytes 11534336 | tf_op jit(solution)/shard_map/all_to_all | solution.py:38
  359.6 388.7 %all-gather.14.cloned.1.call-start = ((), (), s32[]{:S(2)}) async-start(), calls=%async_computation.9 | async-start | bytes 5242880 | tf_op jit(solution)/shard_map/all_gather | solution.py:74
  359.7 131.1 %copy-start.6 = (f32[1408,512]{1,0:T(8,128)S(1)}, f32[1408,512]{1,0:T(8,128)}, u32[]{:S(2)}) copy-start(f32[1408,512]{1,0:T(8,128)} %param.15) | copy-start | bytes 8650756
  483.7 4.3 copy-start.1
  490.7 306.5 %all-gather.18.cloned.1.call-start = ((), (), s32[]{:S(2)}) async-start(), calls=%async_computation.11 | async-start | bytes 7208960 | tf_op jit(solution)/shard_map/all_gather | solution.py:35
  575.0 222.2 %all-to-all-start.3 = ((bf16[512,4,1408]{2,0,1:T(8,128)(2,1)}), bf16[512,4,1408]{2,0,1:T(8,128)(2,1)}, u32[]{:S(2)}, u32[]{:S(2)}) async-start(bf16[512,4,1408]{2,0,1:T(8,128)(2,1)} %bitcast.71), calls=%async_computation.4 | async-start | bytes 11534336 | tf_op jit(solution)/shard_map/all_to_all | solution.py:39
  580.2 314.6 %reduce-scatter.5.cloned.1.call-start = ((), (), s32[]{:S(2)}) async-start(), calls=%async_computation.12 | async-start | bytes 5242880 | tf_op jit(solution)/shard_map/reduce_scatter | solution.py:76
  817.8 77.0 %copy-start = (bf16[256,2048]{1,0:T(8,128)(2,1)S(1)}, bf16[256,2048]{1,0:T(8,128)(2,1)}, u32[]{:S(2)}) copy-start(bf16[256,2048]{1,0:T(8,128)(2,1)} %multiply_convert_fusion.5) | copy-start | bytes 3145732
  894.7 3.7 copy-start.2
  899.9 11.5 %slice-start = ((s8[5767168]{0:T(1024)(128)(4,1)}), s8[4194304]{0:T(1024)(128)(4,1)S(1)}, s32[]{:S(2)}) async-start(s8[5767168]{0:T(1024)(128)(4,1)} %bitcast.69), calls=%async_computation.15 | async-start | bytes 8388608
  905.7 5.7 slice-start.1
  913.9 11.5 %slice-start.2 = ((s8[5767168]{0:T(1024)(128)(4,1)}), s8[4194304]{0:T(1024)(128)(4,1)S(1)}, s32[]{:S(2)}) async-start(s8[5767168]{0:T(1024)(128)(4,1)} %bitcast.73), calls=%async_computation.17 | async-start | bytes 8388608
  919.7 5.7 slice-start.3
  (1 other events, 3.3 us)
Sparse Core Ops, SparseCore 0:
  10.6 46.0 all-gather.9
  58.8 43.3 all-gather.19
  104.4 43.3 all-gather.11
  205.2 43.7 all-gather.15
  348.4 135.2 reduce-scatter.2
  485.7 89.2 all-gather.21
  577.1 171.1 all-gather.13
  750.4 46.6 all-gather.17
  817.9 76.7 reduce-scatter.4
